TPU v7x, 32 devices: a whole 2x2x4 slice. The times are simulated.
32 devices in a mesh: fs: 8 (over z, x), tp: 4 (over y, core).
Axes of the slice: x: 2, y: 2, z: 4, core: 2. Of those that a mesh axis runs over, the one named last changes fastest.
Arguments:
- tokens: bfloat16 [8192, 2048], P(('fs', 'tp')), may hold values from -130 to 130
- pool_weight: bfloat16 [4, 512, 512], P(None, 'fs'), may hold values from -0.25 to 0.25
- pool_scale: float32 [2048], replicated, may hold values from 0.5 to 1.5
- gain_mix: float32 [2048], replicated, may hold values from 0.1 to 1.9
- gain_mlp: float32 [2048], replicated, may hold values from 0.1 to 1.9
- w_up: bfloat16 [8192, 2048], P('tp', 'fs'), may hold values from -0.125 to 0.125
- w_down: bfloat16 [8192, 2048], P('tp', 'fs'), may hold values from -0.0625 to 0.0625
- gain_out: float32 [2048], P('tp'), may hold values from 0.1 to 1.9
Outputs:
- result: bfloat16 [8192, 2048], P('fs', 'tp')
All inputs are finite; a program needn't handle non-finite values.
Results may differ from a plain program's by a relative error of at most 0.013.
Values may be sent and summed in bfloat16 or wider, within the bound.
A program may use at most 64 MiB of HBM per device.

v0:
```python
import jax
import jax.numpy as jnp
from jax import lax
from jax.sharding import PartitionSpec as P

D = 2048
SEQ_LEN = 1024
EPS = 1e-06
WINDOWS = (2, 4, 8, 16)


def extended_2(x, sides, width):
    for axis, dim in sides:
        peers, length = (lax.axis_size(axis), x.shape[dim])
        up = [(i, (i + 1) % peers) for i in range(peers - 1)]
        down = [(j, i) for i, j in up]
        last = lax.slice_in_dim(x, length - width, length, axis=dim)
        first = lax.slice_in_dim(x, 0, width, axis=dim)
        before = lax.ppermute(last, axis, up)
        after = lax.ppermute(first, axis, down)
        x = jnp.concatenate([before, x, after], axis=dim)
    return x


def rms_scale(values, gain):
    return values * lax.rsqrt(jnp.mean(values * values, axis=-1, keepdims=True) + EPS) * gain


def local(tokens, pool_weight, pool_scale, gain_mix, gain_mlp, w_up, w_down, gain_out):
    rows = tokens.shape[0]
    width = tokens.shape[1]
    group = width // 4
    offset = lax.axis_index("tp") * rows
    inputs = tokens.astype(jnp.float32)
    normed = rms_scale(inputs, gain_mix).astype(jnp.bfloat16)
    extended = extended_2(normed, (("tp", 0),), 8).astype(jnp.float32)
    line = jnp.arange(rows + 16, dtype=jnp.int32)
    lower_open = offset % SEQ_LEN != 0
    upper_open = (offset + rows) % SEQ_LEN != 0
    keep = jnp.where(line < 8, lower_open, jnp.where(line >= rows + 8, upper_open, True))
    level = extended * keep.astype(jnp.float32)[:, None]
    position = (offset + jnp.arange(rows, dtype=jnp.int32)) % SEQ_LEN
    normed_f32 = normed.astype(jnp.float32)
    full_pool = lax.all_gather(pool_weight, "fs", axis=1, tiled=True)
    pieces = []
    for index, reach in enumerate(WINDOWS):
        half = reach // 2
        level = level[:-half] + level[half:]
        start = 8 - half
        window = level[start : start + rows, :group]
        lower = jnp.maximum(position - half, 0)
        upper = jnp.minimum(position + half, SEQ_LEN)
        counts = (upper - lower).astype(jnp.float32)[:, None]
        own = normed_f32[:, index * group : (index + 1) * group]
        pooled = (window / counts - own).astype(jnp.bfloat16)
        pieces.append(jnp.dot(pooled, full_pool[index], preferred_element_type=jnp.float32))
        level = level[:, group:]
    mixed = jnp.concatenate(pieces, axis=1) * pool_scale
    first_sum = (inputs + mixed).astype(jnp.bfloat16)
    inner = rms_scale(first_sum.astype(jnp.float32), gain_mlp).astype(jnp.bfloat16)
    all_inner = lax.all_gather(inner, "tp", axis=0, tiled=True)
    contract = (((1,), (1,)), ((), ()))
    pre = lax.dot_general(
        all_inner,
        lax.all_gather(w_up, "fs", axis=1, tiled=True),
        contract,
        preferred_element_type=jnp.float32,
    )
    hidden = jnp.square(jax.nn.relu(pre)).astype(jnp.bfloat16)
    partial_terms = jnp.dot(
        hidden, lax.all_gather(w_down, "fs", axis=1, tiled=True), preferred_element_type=jnp.float32
    )
    channel_out = lax.psum_scatter(
        partial_terms.astype(jnp.bfloat16), "tp", scatter_dimension=1, tiled=True
    ).astype(jnp.float32)
    first_columns = lax.all_to_all(first_sum, "tp", split_axis=1, concat_axis=0, tiled=True)
    second_sum = first_columns.astype(jnp.float32) + channel_out
    squares = lax.psum(jnp.sum(second_sum * second_sum, axis=1), "tp")
    scaled = second_sum * lax.rsqrt(squares / D + EPS)[:, None] * gain_out
    return scaled.astype(jnp.bfloat16)


def solution(mesh):
    return jax.shard_map(
        local,
        mesh=mesh,
        in_specs=(
            P(("fs", "tp"), None),
            P(None, "fs", None),
            P(),
            P(),
            P(),
            P("tp", "fs"),
            P("tp", "fs"),
            P("tp"),
        ),
        out_specs=P("fs", "tp"),
        check_vma=False,
    )
```

profile of v0, /device:TPU:0, one launch (start us, length us, event | category | flops | bytes accessed | tf_op | source)
XLA Modules:
  0.0 437.5 jit_solution(9384960922146906074)
XLA Ops:
  6.5 0.7 all-gather.5.cloned.1.call-update
  7.3 1.5 fusion.3
  8.8 2.9 fusion.30
  11.7 2.4 collective-permute-start
  14.1 1.3 collective-permute-start.1
  15.5 3.8 collective-permute-done.1
  19.3 0.2 convert_multiply_fusion.4
  19.5 0.3 slice_add_fusion
  19.8 0.2 slice_add_fusion.1
  20.1 1.2 copy-done.1
  21.4 1.1 fusion.32
  22.6 38.8 %all-gather.5.cloned.1.call-done = bf16[4,512,512]{2,1,0:T(8,128)(2,1)} async-done(((bf16[4,64,512]{2,1,0:T(8,128)(2,1)}), bf16[4,512,512]{2,1,0:T(8,128)(2,1)}) %all-gather.5.cloned.1.call-update) | async-done | bytes 2097168 | tf_op jit(solution)/shard_map/all_gather | solution.py:44
  61.3 1.7 fusion.14
  63.1 0.2 copy-done.3
  63.2 1.7 fusion.12
  65.0 0.4 fusion.10
  65.4 0.6 copy-done.4
  66.2 0.4 fusion.7
  66.7 0.5 fusion
  67.2 0.2 copy-done.7
  67.4 1.3 fusion.2
  68.7 0.7 all-gather.9.cloned.1.call-update
  69.5 0.5 all-gather.11.cloned.1.call-update
  70.0 31.8 %all-gather.7.cloned.1.call-done = bf16[1024,2048]{1,0:T(8,128)(2,1)} async-done(((bf16[256,2048]{1,0:T(8,128)(2,1)}), bf16[1024,2048]{1,0:T(8,128)(2,1)}) %all-gather.7.cloned.1.call-update) | async-done | bytes 4194320 | tf_op jit(solution)/shard_map/all_gather | solution.py:61
  101.8 127.0 %all-gather.9.cloned.1.call-done = bf16[2048,2048]{1,0:T(8,128)(2,1)} async-done(((bf16[2048,256]{1,0:T(8,128)(2,1)}), bf16[2048,2048]{1,0:T(8,128)(2,1)}) %all-gather.9.cloned.1.call-update) | async-done | bytes 8388624 | tf_op jit(solution)/shard_map/all_gather | solution.py:65
  228.8 125.0 %all-gather.11.cloned.1.call-done = bf16[2048,2048]{1,0:T(8,128)(2,1)} async-done(((bf16[2048,256]{1,0:T(8,128)(2,1)}), bf16[2048,2048]{1,0:T(8,128)(2,1)}) %all-gather.11.cloned.1.call-update) | async-done | bytes 8388624 | tf_op jit(solution)/shard_map/all_gather | solution.py:71
  353.9 25.5 %convolution_convert_fusion = bf16[1024,2048]{1,0:T(8,128)(2,1)} fusion(bf16[2048,2048]{1,0:T(8,128)(2,1)} %all-gather.11.cloned.1.call-done, bf16[1024,2048]{1,0:T(8,128)(2,1)} %all-gather.7.cloned.1.call-done, bf16[2048,2048]{1,0:T(8,128)(2,1)} %all-gather.9.cloned.1.call-done), kind=kOutput, calls=%fused_computation.1 | convolution fusion | flops 17188257792 | bytes 25165824 | tf_op jit(solution)/shard_map/dot_general | solution.py:70
  379.5 17.0 %all_to_all.13 = bf16[256,4,512]{2,0,1:T(8,128)(2,1)S(1)} all-to-all(bf16[256,4,512]{2,0,1:T(8,128)(2,1)S(1)} %bitcast.28), channel_id=1, replica_groups=mesh['fs'=8,'tp'=4] {'tp'}, dimensions={1} | all-to-all | bytes 2097152 | tf_op jit(solution)/shard_map/all_to_all | solution.py:76
  396.5 25.6 %reduce-scatter.2.cloned.1.call-done = bf16[1024,512]{1,0:T(8,128)(2,1)} async-done(((bf16[1024,2048]{1,0:T(8,128)(2,1)}), bf16[1024,512]{1,0:T(8,128)(2,1)}) %reduce-scatter.2.cloned.1.call-update) | async-done | bytes 1048592 | tf_op jit(solution)/shard_map/reduce_scatter | solution.py:73
  422.1 1.7 multiply_reduce_fusion
  423.8 5.8 %psum.7 = f32[1024]{0:T(1024)S(1)} all-reduce(f32[1024]{0:T(1024)S(1)} %multiply_reduce_fusion), channel_id=1, replica_groups=mesh['fs'=8,'tp'=4] {'tp'}, use_global_device_ids=true, to_apply=%region_4.5 | all-reduce | flops 1024 | bytes 8192 | tf_op jit(solution)/shard_map/psum | solution.py:78
  429.6 1.4 multiply_convert_fusion.1
  (33 shorter events, 0.9 us)
Async XLA Ops:
  6.5 54.8 %all-gather.5.cloned.1.call-start = ((), (), s32[]{:S(2)}) async-start(), calls=%async_computation.2 | async-start | bytes 2359296 | tf_op jit(solution)/shard_map/all_gather | solution.py:44
  7.3 94.6 %all-gather.7.cloned.1.call-start = ((), (), s32[]{:S(2)}) async-start(), calls=%async_computation.3 | async-start | bytes 5242880 | tf_op jit(solution)/shard_map/all_gather | solution.py:61
  11.7 3.8 collective-permute-start
  14.1 5.2 %collective-permute-start.1 = (bf16[8,2048]{1,0:T(8,128)(2,1)S(1)}, bf16[8,2048]{1,0:T(8,128)(2,1)S(1)}, u32[]{:S(2)}, u32[]{:S(2)}) collective-permute-start(bf16[8,2048]{1,0:T(8,128)(2,1)S(1)} %get-tuple-element.12), channel_id=1, source_target_pairs={{1,0},{2,1},{3,2},{5,4},{6,5},{7,6},{9,8},{10,9},{11,10},{13,12},{... | collective-permute-start | bytes 98312 | tf_op jit(solution)/shard_map/ppermute | solution.py:20
  20.1 1.2 copy-start.1
  61.3 1.9 copy-start.3
  63.0 2.0 copy-start.9
  64.9 1.1 copy-start.4
  64.9 1.2 copy-start.5
  65.4 1.3 copy-start
  65.4 1.3 copy-start.6
  66.7 0.7 copy-start.7
  68.7 160.2 %all-gather.9.cloned.1.call-start = ((), (), s32[]{:S(2)}) async-start(), calls=%async_computation.4 | async-start | bytes 9437184 | tf_op jit(solution)/shard_map/all_gather | solution.py:65
  69.4 284.5 %all-gather.11.cloned.1.call-start = ((), (), s32[]{:S(2)}) async-start(), calls=%async_computation.5 | async-start | bytes 9437184 | tf_op jit(solution)/shard_map/all_gather | solution.py:71
  70.0 352.1 %reduce-scatter.2.cloned.1.call-start = ((), (), s32[]{:S(2)}) async-start(), calls=%async_computation.6 | async-start | bytes 5242880 | tf_op jit(solution)/shard_map/reduce_scatter | solution.py:73
  379.5 50.1 %copy-start.8 = (f32[512]{0:T(512)S(1)}, f32[512]{0:T(512)}, u32[]{:S(2)}) copy-start(f32[512]{0:T(512)} %param.15) | copy-start | bytes 6148
  422.1 7.5 %copy-start.2 = (bf16[1024,512]{1,0:T(8,128)(2,1)S(1)}, bf16[1024,512]{1,0:T(8,128)(2,1)}, u32[]{:S(2)}) copy-start(bf16[1024,512]{1,0:T(8,128)(2,1)} %reduce-scatter.2.cloned.1.call-done) | copy-start | bytes 3145732
Sparse Core Ops, SparseCore 0:
  9.5 51.7 all-gather.4
  68.8 32.9 all-gather.6
  103.9 124.9 all-gather.8
  230.7 123.1 all-gather.10
  379.5 42.5 reduce-scatter.1
where the time goes:
time: 438 us
  waiting for transfers between devices  354 us (81%)
  matrix products  29.5 us (7%)
  blocking collectives  22.8 us (5%)
  between operations  13.3 us (3%)
  other arithmetic  10.2 us (2%)
    all_gather x1, waiting for transfers between devices, local(): lax.all_gather(w_up, 'fs', axis=1, tiled=True)  127 us
    all_gather x1, waiting for transfers between devices, local(): lax.all_gather(w_down, 'fs', axis=1, tiled=True)  125 us
    all_gather x1, waiting for transfers between devices, local(): full_pool = lax.all_gather(pool_weight, 'fs', axis=1, tiled=True)  38.8 us
    all_gather x1, waiting for transfers between devices, local(): all_inner = lax.all_gather(inner, 'tp', axis=0, tiled=True)  31.8 us
    reduce_scatter x1, waiting for transfers between devices, local(): lax.psum_scatter(partial_terms.astype(jnp.bfloat16), 'tp', scatter_dimens...  25.6 us
    dot_general x1, matrix products, local(): jnp.dot(hidden, lax.all_gather(w_down, 'fs', axis=1, tiled=True), preferr...  25.5 us
    all_to_all x1, blocking collectives, local(): lax.all_to_all(first_sum, 'tp', split_axis=1, concat_axis=0, tiled=True)  17 us
  transfers between devices with their start and end apart: 7, of which 6 were waited for; matrix products, arithmetic and copies ran while one was open for 1% of the time, Pallas kernels for 0%

commit v1 on v0

--- a/solution.py
+++ b/solution.py
@@ -41,7 +41,14 @@
     level = extended * keep.astype(jnp.float32)[:, None]
     position = (offset + jnp.arange(rows, dtype=jnp.int32)) % SEQ_LEN
     normed_f32 = normed.astype(jnp.float32)
-    full_pool = lax.all_gather(pool_weight, "fs", axis=1, tiled=True)
+    size = lax.axis_size("fs")
+    right = [(i_2, (i_2 + 1) % size) for i_2 in range(size)]
+    shards = [pool_weight]
+    for reach_2 in range(1, size):
+        shards = [lax.ppermute(shards[0], "fs", right), *shards]
+    result = jnp.concatenate(shards, axis=1)
+    places = (lax.axis_index("fs") + 1) * shards[-1].shape[1]
+    full_pool = jnp.roll(result, places, axis=1)
     pieces = []
     for index, reach in enumerate(WINDOWS):
         half = reach // 2

time: 438 us -> 451 us (1.030)
  waiting for transfers between devices: 354 us -> 368 us
    ppermute x0 -> x7, waiting for transfers between devices: none -> 58.6 us  [local(): shards = [lax.ppermute(shards[0], 'fs', right), *shards]]
    all_gather x1 -> x0, waiting for transfers between devices: 38.8 us -> none  [local(): full_pool = lax.all_gather(pool_weight, 'fs', axis=1, tiled=True)]
  transfers between devices with their start and end apart: 7 -> 13, of which waited for: 6 -> 11; matrix products, arithmetic and copies ran while one was open for 1% -> 1% of each run, Pallas kernels for 0% -> 0%
where the time goes in v1:
time: 451 us; the launch traced here: 450 us
  waiting for transfers between devices  368 us (82%)
  matrix products  26.9 us (6%)
  blocking collectives  22.8 us (5%)
  between operations  13.4 us (3%)
  other arithmetic  9.56 us (2%)
  starting transfers between devices  5.85 us (1%)
    all_gather x1, waiting for transfers between devices, local(): lax.all_gather(w_up, 'fs', axis=1, tiled=True)  127 us
    all_gather x1, waiting for transfers between devices, local(): lax.all_gather(w_down, 'fs', axis=1, tiled=True)  125 us
    ppermute x7, waiting for transfers between devices, local(): shards = [lax.ppermute(shards[0], 'fs', right), *shards]  58.6 us
    all_gather x1, waiting for transfers between devices, local(): all_inner = lax.all_gather(inner, 'tp', axis=0, tiled=True)  30.2 us
    reduce_scatter x1, waiting for transfers between devices, local(): lax.psum_scatter(partial_terms.astype(jnp.bfloat16), 'tp', scatter_dimens...  25.6 us
    dot_general x1, matrix products, local(): jnp.dot(hidden, lax.all_gather(w_down, 'fs', axis=1, tiled=True), preferr...  25.4 us
    all_to_all x1, blocking collectives, local(): lax.all_to_all(first_sum, 'tp', split_axis=1, concat_axis=0, tiled=True)  17 us
  transfers between devices with their start and end apart: 13, of which 11 were waited for; matrix products, arithmetic and copies ran while one was open for 1% of the time, Pallas kernels for 0%

profile of v1, /device:TPU:0, one launch (start us, length us, event | category | flops | bytes accessed | tf_op | source)
XLA Modules:
  0.0 450.3 jit_solution(7362654987262233278)
XLA Ops:
  6.5 3.0 collective-permute-start.2
  9.5 1.5 fusion.3
  11.0 1.6 fusion.34
  12.6 1.5 collective-permute-start
  14.1 1.3 collective-permute-start.1
  15.4 3.7 collective-permute-done.2
  19.1 0.6 subtract_convert_fusion
  19.7 9.6 %collective-permute-done.3 = bf16[4,64,512]{2,1,0:T(8,128)(2,1)} collective-permute-done((bf16[4,64,512]{2,1,0:T(8,128)(2,1)S(1)}, bf16[4,64,512]{2,1,0:T(8,128)(2,1)}, u32[]{:S(2)}, u32[]{:S(2)}) %collective-permute-start.3) | collective-permute-done | bytes 262176 | tf_op jit(solution)/shard_map/ppermute | solution.py:48
  29.6 9.3 %collective-permute-done.4 = bf16[4,64,512]{2,1,0:T(8,128)(2,1)S(1)} collective-permute-done((bf16[4,64,512]{2,1,0:T(8,128)(2,1)}, bf16[4,64,512]{2,1,0:T(8,128)(2,1)S(1)}, u32[]{:S(2)}, u32[]{:S(2)}) %collective-permute-start.4) | collective-permute-done | bytes 262176 | tf_op jit(solution)/shard_map/ppermute | solution.py:48
  38.9 0.4 slice_add_fusion
  39.2 8.7 %collective-permute-done.5 = bf16[4,64,512]{2,1,0:T(8,128)(2,1)S(1)} collective-permute-done((bf16[4,64,512]{2,1,0:T(8,128)(2,1)S(1)}, bf16[4,64,512]{2,1,0:T(8,128)(2,1)S(1)}, u32[]{:S(2)}, u32[]{:S(2)}) %collective-permute-start.5) | collective-permute-done | bytes 262176 | tf_op jit(solution)/shard_map/ppermute | solution.py:48
  48.2 8.8 %collective-permute-done.6 = bf16[4,64,512]{2,1,0:T(8,128)(2,1)S(1)} collective-permute-done((bf16[4,64,512]{2,1,0:T(8,128)(2,1)S(1)}, bf16[4,64,512]{2,1,0:T(8,128)(2,1)S(1)}, u32[]{:S(2)}, u32[]{:S(2)}) %collective-permute-start.6) | collective-permute-done | bytes 262176 | tf_op jit(solution)/shard_map/ppermute | solution.py:48
  57.2 9.5 %collective-permute-done.7 = bf16[4,64,512]{2,1,0:T(8,128)(2,1)S(1)} collective-permute-done((bf16[4,64,512]{2,1,0:T(8,128)(2,1)S(1)}, bf16[4,64,512]{2,1,0:T(8,128)(2,1)S(1)}, u32[]{:S(2)}, u32[]{:S(2)}) %collective-permute-start.7) | collective-permute-done | bytes 262176 | tf_op jit(solution)/shard_map/ppermute | solution.py:48
  66.8 8.9 %collective-permute-done.8 = bf16[4,64,512]{2,1,0:T(8,128)(2,1)S(1)} collective-permute-done((bf16[4,64,512]{2,1,0:T(8,128)(2,1)S(1)}, bf16[4,64,512]{2,1,0:T(8,128)(2,1)S(1)}, u32[]{:S(2)}, u32[]{:S(2)}) %collective-permute-start.8) | collective-permute-done | bytes 262176 | tf_op jit(solution)/shard_map/ppermute | solution.py:48
  75.9 1.0 constant_dynamic-update-slice_fusion.10
  77.0 1.0 constant_dynamic-update-slice_fusion.2
  78.1 0.4 fusion.14
  78.5 0.4 fusion.12
  79.9 0.8 copy-done
  80.7 0.5 fusion
  81.4 1.3 fusion.2
  82.8 0.7 all-gather.6.cloned.1.call-update
  83.5 0.7 all-gather.8.cloned.1.call-update
  84.3 30.2 %all-gather.4.cloned.1.call-done = bf16[1024,2048]{1,0:T(8,128)(2,1)} async-done(((bf16[256,2048]{1,0:T(8,128)(2,1)}), bf16[1024,2048]{1,0:T(8,128)(2,1)}) %all-gather.4.cloned.1.call-update) | async-done | bytes 4194320 | tf_op jit(solution)/shard_map/all_gather | solution.py:68
  114.4 127.0 %all-gather.6.cloned.1.call-done = bf16[2048,2048]{1,0:T(8,128)(2,1)} async-done(((bf16[2048,256]{1,0:T(8,128)(2,1)}), bf16[2048,2048]{1,0:T(8,128)(2,1)}) %all-gather.6.cloned.1.call-update) | async-done | bytes 8388624 | tf_op jit(solution)/shard_map/all_gather | solution.py:72
  241.4 125.2 %all-gather.8.cloned.1.call-done = bf16[2048,2048]{1,0:T(8,128)(2,1)} async-done(((bf16[2048,256]{1,0:T(8,128)(2,1)}), bf16[2048,2048]{1,0:T(8,128)(2,1)}) %all-gather.8.cloned.1.call-update) | async-done | bytes 8388624 | tf_op jit(solution)/shard_map/all_gather | solution.py:78
  366.6 25.4 %convolution_convert_fusion = bf16[1024,2048]{1,0:T(8,128)(2,1)} fusion(bf16[2048,2048]{1,0:T(8,128)(2,1)} %all-gather.8.cloned.1.call-done, bf16[1024,2048]{1,0:T(8,128)(2,1)} %all-gather.4.cloned.1.call-done, bf16[2048,2048]{1,0:T(8,128)(2,1)} %all-gather.6.cloned.1.call-done), kind=kOutput, calls=%fused_computation.1 | convolution fusion | flops 17188257792 | bytes 25165824 | tf_op jit(solution)/shard_map/dot_general | solution.py:77
  392.2 17.0 %all_to_all.13 = bf16[256,4,512]{2,0,1:T(8,128)(2,1)S(1)} all-to-all(bf16[256,4,512]{2,0,1:T(8,128)(2,1)S(1)} %bitcast.28), channel_id=1, replica_groups=mesh['fs'=8,'tp'=4] {'tp'}, dimensions={1} | all-to-all | bytes 2097152 | tf_op jit(solution)/shard_map/all_to_all | solution.py:83
  409.2 25.6 %reduce-scatter.2.cloned.1.call-done = bf16[1024,512]{1,0:T(8,128)(2,1)} async-done(((bf16[1024,2048]{1,0:T(8,128)(2,1)}), bf16[1024,512]{1,0:T(8,128)(2,1)}) %reduce-scatter.2.cloned.1.call-update) | async-done | bytes 1048592 | tf_op jit(solution)/shard_map/reduce_scatter | solution.py:80
  434.9 1.7 multiply_reduce_fusion
  436.6 5.8 %psum.7 = f32[1024]{0:T(1024)S(1)} all-reduce(f32[1024]{0:T(1024)S(1)} %multiply_reduce_fusion), channel_id=1, replica_groups=mesh['fs'=8,'tp'=4] {'tp'}, use_global_device_ids=true, to_apply=%region_4.5 | all-reduce | flops 1024 | bytes 8192 | tf_op jit(solution)/shard_map/psum | solution.py:85
  442.4 1.4 multiply_convert_fusion.1
  (54 shorter events, 2.5 us)
Async XLA Ops:
  6.5 107.9 %all-gather.4.cloned.1.call-start = ((), (), s32[]{:S(2)}) async-start(), calls=%async_computation.2 | async-start | bytes 5242880 | tf_op jit(solution)/shard_map/all_gather | solution.py:68
  6.5 12.5 %collective-permute-start.2 = (bf16[4,64,512]{2,1,0:T(8,128)(2,1)}, bf16[4,64,512]{2,1,0:T(8,128)(2,1)S(1)}, u32[]{:S(2)}, u32[]{:S(2)}) collective-permute-start(bf16[4,64,512]{2,1,0:T(8,128)(2,1)} %param.9), channel_id=1, source_target_pairs={{0,4},{4,8},{8,12},{12,16},{16,20},{20,24},{24,28},{28,0},{1,5},{5... | collective-permute-start | bytes 786440 | tf_op jit(solution)/shard_map/ppermute | solution.py:48
  12.6 16.7 %collective-permute-start = (bf16[8,2048]{1,0:T(8,128)(2,1)S(1)}, bf16[8,2048]{1,0:T(8,128)(2,1)S(1)}, u32[]{:S(2)}, u32[]{:S(2)}) collective-permute-start(bf16[8,2048]{1,0:T(8,128)(2,1)S(1)} %get-tuple-element.11), channel_id=1, source_target_pairs={{0,1},{1,2},{2,3},{4,5},{5,6},{6,7},{8,9},{9,10},{10,11},{12,13},{... | collective-permute-start | bytes 98312 | tf_op jit(solution)/shard_map/ppermute | solution.py:19
  14.1 15.3 %collective-permute-start.1 = (bf16[8,2048]{1,0:T(8,128)(2,1)S(1)}, bf16[8,2048]{1,0:T(8,128)(2,1)S(1)}, u32[]{:S(2)}, u32[]{:S(2)}) collective-permute-start(bf16[8,2048]{1,0:T(8,128)(2,1)S(1)} %get-tuple-element.12), channel_id=1, source_target_pairs={{1,0},{2,1},{3,2},{5,4},{6,5},{7,6},{9,8},{10,9},{11,10},{13,12},{... | collective-permute-start | bytes 98312 | tf_op jit(solution)/shard_map/ppermute | solution.py:20
  19.1 10.3 %collective-permute-start.3 = (bf16[4,64,512]{2,1,0:T(8,128)(2,1)S(1)}, bf16[4,64,512]{2,1,0:T(8,128)(2,1)}, u32[]{:S(2)}, u32[]{:S(2)}) collective-permute-start(bf16[4,64,512]{2,1,0:T(8,128)(2,1)S(1)} %collective-permute-done.2), channel_id=1, source_target_pairs={{0,4},{4,8},{8,12},{12,16},{16,20},{20,24},{24,28},{28,0},{1,5},{5... | collective-permute-start | bytes 786440 | tf_op jit(solution)/shard_map/ppermute | solution.py:48
  29.3 9.5 %collective-permute-start.4 = (bf16[4,64,512]{2,1,0:T(8,128)(2,1)}, bf16[4,64,512]{2,1,0:T(8,128)(2,1)S(1)}, u32[]{:S(2)}, u32[]{:S(2)}) collective-permute-start(bf16[4,64,512]{2,1,0:T(8,128)(2,1)} %collective-permute-done.3), channel_id=1, source_target_pairs={{0,4},{4,8},{8,12},{12,16},{16,20},{20,24},{24,28},{28,0},{1,5},{5... | collective-permute-start | bytes 786440 | tf_op jit(solution)/shard_map/ppermute | solution.py:48
  38.9 9.1 %collective-permute-start.5 = (bf16[4,64,512]{2,1,0:T(8,128)(2,1)S(1)}, bf16[4,64,512]{2,1,0:T(8,128)(2,1)S(1)}, u32[]{:S(2)}, u32[]{:S(2)}) collective-permute-start(bf16[4,64,512]{2,1,0:T(8,128)(2,1)S(1)} %collective-permute-done.4), channel_id=1, source_target_pairs={{0,4},{4,8},{8,12},{12,16},{16,20},{20,24},{24,28},{28,0},{1,5},{5... | collective-permute-start | bytes 786440 | tf_op jit(solution)/shard_map/ppermute | solution.py:48
  47.9 9.1 %collective-permute-start.6 = (bf16[4,64,512]{2,1,0:T(8,128)(2,1)S(1)}, bf16[4,64,512]{2,1,0:T(8,128)(2,1)S(1)}, u32[]{:S(2)}, u32[]{:S(2)}) collective-permute-start(bf16[4,64,512]{2,1,0:T(8,128)(2,1)S(1)} %collective-permute-done.5), channel_id=1, source_target_pairs={{0,4},{4,8},{8,12},{12,16},{16,20},{20,24},{24,28},{28,0},{1,5},{5... | collective-permute-start | bytes 786440 | tf_op jit(solution)/shard_map/ppermute | solution.py:48
  57.0 9.7 %collective-permute-start.7 = (bf16[4,64,512]{2,1,0:T(8,128)(2,1)S(1)}, bf16[4,64,512]{2,1,0:T(8,128)(2,1)S(1)}, u32[]{:S(2)}, u32[]{:S(2)}) collective-permute-start(bf16[4,64,512]{2,1,0:T(8,128)(2,1)S(1)} %collective-permute-done.6), channel_id=1, source_target_pairs={{0,4},{4,8},{8,12},{12,16},{16,20},{20,24},{24,28},{28,0},{1,5},{5... | collective-permute-start | bytes 786440 | tf_op jit(solution)/shard_map/ppermute | solution.py:48
  66.7 9.1 %collective-permute-start.8 = (bf16[4,64,512]{2,1,0:T(8,128)(2,1)S(1)}, bf16[4,64,512]{2,1,0:T(8,128)(2,1)S(1)}, u32[]{:S(2)}, u32[]{:S(2)}) collective-permute-start(bf16[4,64,512]{2,1,0:T(8,128)(2,1)S(1)} %collective-permute-done.7), channel_id=1, source_target_pairs={{0,4},{4,8},{8,12},{12,16},{16,20},{20,24},{24,28},{28,0},{1,5},{5... | collective-permute-start | bytes 786440 | tf_op jit(solution)/shard_map/ppermute | solution.py:48
  66.8 10.1 %copy-start.2 = (bf16[4,64,512]{2,1,0:T(8,128)(2,1)S(1)}, bf16[4,64,512]{2,1,0:T(8,128)(2,1)}, u32[]{:S(2)}) copy-start(bf16[4,64,512]{2,1,0:T(8,128)(2,1)} %param.9) | copy-start | bytes 786436
  78.4 0.7 copy-start.6
  79.5 1.2 copy-start
  79.5 1.2 copy-start.3
  80.7 0.7 copy-start.4
  82.7 158.7 %all-gather.6.cloned.1.call-start = ((), (), s32[]{:S(2)}) async-start(), calls=%async_computation.3 | async-start | bytes 9437184 | tf_op jit(solution)/shard_map/all_gather | solution.py:72
  83.5 283.2 %all-gather.8.cloned.1.call-start = ((), (), s32[]{:S(2)}) async-start(), calls=%async_computation.4 | async-start | bytes 9437184 | tf_op jit(solution)/shard_map/all_gather | solution.py:78
  84.2 350.7 %reduce-scatter.2.cloned.1.call-start = ((), (), s32[]{:S(2)}) async-start(), calls=%async_computation.5 | async-start | bytes 5242880 | tf_op jit(solution)/shard_map/reduce_scatter | solution.py:80
  392.2 50.2 %copy-start.5 = (f32[512]{0:T(512)S(1)}, f32[512]{0:T(512)}, u32[]{:S(2)}) copy-start(f32[512]{0:T(512)} %param.15) | copy-start | bytes 6148
  434.9 7.5 %copy-start.1 = (bf16[1024,512]{1,0:T(8,128)(2,1)S(1)}, bf16[1024,512]{1,0:T(8,128)(2,1)}, u32[]{:S(2)}) copy-start(bf16[1024,512]{1,0:T(8,128)(2,1)} %reduce-scatter.2.cloned.1.call-done) | copy-start | bytes 3145732
Sparse Core Ops, SparseCore 0:
  82.8 31.5 all-gather.3
  116.5 124.9 all-gather.5
  243.5 123.1 all-gather.7
  392.2 42.5 reduce-scatter.1
